TPU v7x, 1024 devices: a whole 4x8x16 slice. The times are simulated.
1024 devices in a mesh: gr: 2 (over z_hi), sp: 64 (over z_lo, y), tp: 8 (over x, core).
Axes of the slice: x: 4, y: 8, z: 16 (z_hi: 2, z_lo: 8; z = z_hi * 8 + z_lo), core: 2. Of those that a mesh axis runs over, the one named last changes fastest.
Arguments:
- layer_input: bfloat16 [2, 98304, 2048], P('gr', ('sp', 'tp')), may hold values from -6 to 6
- key_weight: bfloat16 [2048, 2048], P(None, 'tp'), may hold values from -0.125 to 0.125
- value_weight: bfloat16 [2048, 2048], P(None, 'tp'), may hold values from -0.125 to 0.125
- new_queries: bfloat16 [2, 2048], P('gr', 'tp'), may hold values from -280 to 280
- lambdas: float32 [16], P('tp'), may hold values from 0.3 to 0.8
- head_gain: float32 [128], replicated, may hold values from 0.1 to 1.9
- out_weight: bfloat16 [2048, 2048], P('tp'), may hold values from -0.125 to 0.125
Outputs:
- key_cache: bfloat16 [2, 98304, 2048], P('gr', 'sp', 'tp')
- value_cache: bfloat16 [2, 98304, 2048], P('gr', 'sp', 'tp')
- mixed: bfloat16 [2, 2048], P('gr', 'tp')
All inputs are finite; a program needn't handle non-finite values.
Results may differ from a plain program's by a relative error of at most 0.03.
Values may be sent and summed in bfloat16 or wider, within the bound.
A program may use at most 64 MiB of HBM per device.

v0:
```python
import jax
import jax.numpy as jnp
from jax import lax
from jax.sharding import PartitionSpec as P


def copy_for_each(array, axis):
    copies = jnp.broadcast_to(array, (lax.axis_size(axis), *array.shape))
    return lax.all_to_all(copies, axis, split_axis=0, concat_axis=0, tiled=True)


def gathered_once(array, axis):
    leaves = jax.tree.leaves(array)
    turns = sorted(range(len(leaves)), key=lambda k: -leaves[k].size)
    width = (1, *leaves[turns[0]].shape)[-1]
    lines = [
        jnp.pad(leaves[k].reshape(-1), (0, -leaves[k].size % width)).reshape(-1, width)
        for k in turns
    ]
    both, at, found = (copy_for_each(jnp.concatenate(lines), axis), 0, {})
    for k, line in zip(turns, lines):
        section = both[:, at : at + len(line)].reshape(len(both), -1)
        found[k] = section[:, : leaves[k].size].reshape(-1, *leaves[k].shape)
        at += len(line)
    numbers = iter(range(len(leaves)))
    return jax.tree.map(lambda _: found[next(numbers)], array)


def combined_pairwise(pieces, combine):
    while len(jax.tree.leaves(pieces)[0]) > 1:
        pieces = jax.vmap(combine)(
            *(jax.tree.map(lambda part: part[side::2], pieces) for side in (0, 1))
        )
    return jax.tree.map(lambda part: part[0], pieces)


def joined_all(array, axis, combine):
    pieces = gathered_once(array, axis)
    return combined_pairwise(pieces, combine)


def split_up(array, dim, peers):
    shape = array.shape
    blocks = array.reshape(*shape[:dim], peers, shape[dim] // peers, *shape[dim + 1 :])
    return jnp.moveaxis(blocks, dim, 0)


def summed_on_arrival(array, axis, dim):
    peers = lax.axis_size(axis)
    blocks = lax.all_to_all(split_up(array, dim, peers), axis, 0, 0, tiled=True)
    return jnp.sum(blocks.astype(jnp.float32), axis=0)


def rotate(raw_keys, positions, head_dim):
    inverse = 1.0 / 10000.0 ** (jnp.arange(0, head_dim, 2, dtype=jnp.float32) / head_dim)
    angles = positions.astype(jnp.float32)[:, None] * inverse[None, :]
    angles = jnp.concatenate([angles, angles], axis=-1)
    cosine = jnp.cos(angles)[:, None, :]
    sine = jnp.sin(angles)[:, None, :]
    first_half, second_half = jnp.split(raw_keys, 2, axis=-1)
    turned = jnp.concatenate([-second_half, first_half], axis=-1)
    return raw_keys * cosine + turned * sine


def partial_read(queries, key_rows, value_rows, heads_here, head_dim):
    seq_count = queries.shape[0]
    queries_wide = queries.reshape(seq_count, heads_here, 2, head_dim)
    keys_wide = key_rows.reshape(seq_count, -1, heads_here, 2, head_dim)
    scores = jnp.einsum(
        "shmd,slhmd->shml", queries_wide, keys_wide, preferred_element_type=jnp.float32
    )
    scores = scores * head_dim ** (-0.5)
    highest = jnp.max(scores, axis=-1)
    weights = jnp.exp(scores - highest[..., None])
    totals = jnp.sum(weights, axis=-1)
    values_wide = value_rows.reshape(seq_count, -1, heads_here, 2 * head_dim).astype(jnp.float32)
    weighted = jnp.einsum("shml,slhe->shme", weights, values_wide)
    return (highest, totals, weighted)


def combine(earlier, later):
    highest = jnp.maximum(earlier[0], later[0])
    factor_one = jnp.exp(earlier[0] - highest)
    factor_two = jnp.exp(later[0] - highest)
    totals = earlier[1] * factor_one + later[1] * factor_two
    weighted = earlier[2] * factor_one[..., None] + later[2] * factor_two[..., None]
    return (highest, totals, weighted)


def finish(totals, weighted, lambdas, head_gain):
    reads = weighted / totals[..., None]
    diff = reads[:, :, 0] - lambdas[None, :, None] * reads[:, :, 1]
    normed = diff * lax.rsqrt(jnp.mean(diff * diff, axis=-1, keepdims=True) + 1e-06) * head_gain
    return normed.reshape(normed.shape[0], -1).astype(jnp.bfloat16)


def on_device(layer_input, key_weight, value_weight, new_queries, lambdas, head_gain, out_weight):
    heads_here = lambdas.shape[0]
    column_count = key_weight.shape[1]
    head_dim = column_count // (2 * heads_here)
    rows_here = layer_input.shape[1]
    first_position = lax.axis_index("sp") * (rows_here * lax.axis_size("tp"))
    piece = lax.all_gather(layer_input, "tp", axis=1, tiled=True)
    seq_count = piece.shape[0]
    count = piece.shape[1]
    flattened = piece.reshape(seq_count * count, piece.shape[2])
    raw_keys = jnp.dot(flattened, key_weight, preferred_element_type=jnp.float32)
    raw_values = jnp.dot(flattened, value_weight, preferred_element_type=jnp.float32)
    positions = first_position + jnp.arange(count, dtype=jnp.int32)
    turned_keys = rotate(
        raw_keys.reshape(seq_count, count, 2 * heads_here, head_dim), positions, head_dim
    )
    key_part = turned_keys.reshape(seq_count, count, column_count).astype(jnp.bfloat16)
    value_part = raw_values.reshape(seq_count, count, column_count).astype(jnp.bfloat16)
    both = jnp.concatenate([key_part, value_part], axis=2)
    key_rows = both[:, :, :column_count]
    value_rows = both[:, :, column_count:]
    highest, totals, weighted = partial_read(
        new_queries, key_rows, value_rows, heads_here, head_dim
    )
    highest, totals, weighted = joined_all((highest, totals, weighted), "sp", combine)
    headed = finish(totals, weighted, lambdas, head_gain)
    partials = jnp.dot(headed, out_weight, preferred_element_type=jnp.float32)
    partials = partials.astype(jnp.bfloat16).astype(jnp.float32)
    mixed = summed_on_arrival(partials.astype(jnp.bfloat16), "tp", 1).astype(jnp.bfloat16)
    return (key_rows, value_rows, mixed)


def solution(mesh):
    in_specs = (
        P("gr", ("sp", "tp"), None),
        P(None, "tp"),
        P(None, "tp"),
        P("gr", "tp"),
        P("tp"),
        P(),
        P("tp", None),
    )
    out_specs = (P("gr", "sp", "tp"), P("gr", "sp", "tp"), P("gr", "tp"))
    return jax.shard_map(
        on_device, mesh=mesh, in_specs=in_specs, out_specs=out_specs, check_vma=False
    )
```

profile of v0, /device:TPU:1, one launch (start us, length us, event | category | flops | bytes accessed | tf_op | source)
XLA Modules:
  0.0 143.3 jit_solution(9386524889777178618)
XLA Ops:
  7.2 0.7 all-gather.2.cloned.1.call-update
  7.9 0.7 reduce.7
  8.8 1.4 fusion.10
  10.2 61.0 %all-gather.2.cloned.1.call-done = bf16[1,1536,2048]{2,1,0:T(8,128)(2,1)} async-done(((bf16[1,192,2048]{2,1,0:T(8,128)(2,1)}), bf16[1,1536,2048]{2,1,0:T(8,128)(2,1)}) %all-gather.2.cloned.1.call-update) | async-done | bytes 6291472 | tf_op jit(solution)/shard_map/all_gather | solution.py:103
  71.2 4.6 %fusion.2 = f32[1536,256]{0,1:T(8,128)S(1)} fusion(bf16[2048,256]{1,0:T(8,128)(2,1)S(1)} %copy-done, bf16[1,1536,2048]{2,1,0:T(8,128)(2,1)} %all-gather.2.cloned.1.call-done), kind=kOutput, calls=%fused_computation.2 | convolution fusion | flops 1610612736 | bytes 8912896 | tf_op jit(solution)/shard_map/dot_general | solution.py:107
  75.8 0.1 slice_negate_fusion
  76.0 0.1 pad_maximum_fusion
  76.1 0.4 fusion.8
  76.5 0.2 fusion.36
  76.7 0.1 fusion.21
  76.8 0.2 fusion.11
  77.1 4.9 %fusion.4 = bf16[1536,256]{0,1:T(8,128)(2,1)S(1)} fusion(bf16[2048,256]{1,0:T(8,128)(2,1)} %param.9, bf16[1,1536,2048]{2,1,0:T(8,128)(2,1)} %all-gather.2.cloned.1.call-done), kind=kOutput, calls=%fused_computation.4 | convolution fusion | flops 1611005952 | bytes 8126464 | tf_op jit(solution)/shard_map/dot_general | solution.py:108
  82.0 0.8 copy-done.2
  82.8 0.3 fusion.12
  83.3 36.1 %all_to_all.10 = f32[64,6,128]{2,1,0:T(8,128)S(1)} all-to-all(f32[64,6,128]{2,1,0:T(8,128)S(1)} %broadcast_in_dim.2), channel_id=1, replica_groups=mesh['gr'=2,'sp'=64,'tp'=8] {'sp'}, dimensions={0} | all-to-all | bytes 393216 | tf_op jit(solution)/shard_map/all_to_all | solution.py:9
  119.5 0.1 slice.140
  119.7 0.1 slice.139
  119.9 0.1 slice.165
  120.0 0.1 slice.164
  122.9 0.2 fusion.33
  123.1 0.2 multiply_add_fusion
  123.3 0.1 multiply_add_fusion.1
  123.8 0.2 multiply_reduce_fusion
  124.2 0.2 fusion.37
  124.4 0.5 broadcast.130
  124.9 0.7 reduce.14
  125.6 0.6 reshape.339
  126.2 5.0 %all-to-all-start.1 = ((bf16[8,2,128]{2,1,0:T(2,128)(2,1)}), bf16[8,2,128]{2,1,0:T(2,128)(2,1)S(1)}, u32[]{:S(2)}, u32[]{:S(2)}) async-start(bf16[8,2,128]{2,1,0:T(2,128)(2,1)} %reshape.339), calls=%async_computation.1 | async-start | bytes 8192 | tf_op jit(solution)/shard_map/all_to_all | solution.py:50
  131.3 2.3 %copy.66 = bf16[1,1536,256]{2,1,0:T(8,128)(2,1)} copy(bf16[1,1536,256]{1,2,0:T(8,128)(2,1)} %bitcast.95) | data formatting | bytes 1572864
  133.6 1.2 copy.65
  134.7 1.2 all-to-all-done.1
  135.9 0.6 reduce_sum.35
  (72 shorter events, 3.9 us)
Async XLA Ops:
  7.2 64.1 %copy-start = (bf16[2048,256]{1,0:T(8,128)(2,1)S(1)}, bf16[2048,256]{1,0:T(8,128)(2,1)}, u32[]{:S(2)}) copy-start(bf16[2048,256]{1,0:T(8,128)(2,1)} %param.8) | copy-start | bytes 3145732
  7.2 64.0 %all-gather.2.cloned.1.call-start = ((), (), s32[]{:S(2)}) async-start(), calls=%async_computation.2 | async-start | bytes 7077888 | tf_op jit(solution)/shard_map/all_gather | solution.py:103
  82.0 0.9 copy-start.2
  82.0 41.8 %copy-start.4 = (f32[2]{0:T(128)S(1)}, f32[2]{0:T(128)}, u32[]{:S(2)}) copy-start(f32[2]{0:T(128)} %param.11) | copy-start | bytes 28
  82.0 42.1 %copy-start.3 = (f32[128]{0:T(128)S(1)}, f32[128]{0:T(128)}, u32[]{:S(2)}) copy-start(f32[128]{0:T(128)} %param.12) | copy-start | bytes 1540
  82.0 42.1 %copy-start.1 = (bf16[256,2048]{1,0:T(8,128)(2,1)S(1)}, bf16[256,2048]{1,0:T(8,128)(2,1)}, u32[]{:S(2)}) copy-start(bf16[256,2048]{1,0:T(8,128)(2,1)} %param.13) | copy-start | bytes 3145732
  126.2 9.7 %all-to-all-start.1 = ((bf16[8,2,128]{2,1,0:T(2,128)(2,1)}), bf16[8,2,128]{2,1,0:T(2,128)(2,1)S(1)}, u32[]{:S(2)}, u32[]{:S(2)}) async-start(bf16[8,2,128]{2,1,0:T(2,128)(2,1)} %reshape.339), calls=%async_computation.1 | async-start | bytes 8192 | tf_op jit(solution)/shard_map/all_to_all | solution.py:50
Sparse Core Ops, SparseCore 0:
  10.7 60.4 all-gather.1
where the time goes:
time: 144 us; the launch traced here: 143 us
  waiting for transfers between devices  62.9 us (44%)
  blocking collectives  36.1 us (25%)
  between operations  14.3 us (10%)
  matrix products  10.3 us (7%)
  local copies, waits for them, and re-layouts  9.7 us (7%)
  starting transfers between devices  5.08 us (4%)
  other arithmetic  5.04 us (4%)
    all_gather x1, waiting for transfers between devices, on_device(): piece = lax.all_gather(layer_input, 'tp', axis=1, tiled=True)  61 us
    all_to_all x1, blocking collectives, copy_for_each(): return lax.all_to_all(copies, axis, split_axis=0, concat_axis=0, tiled=True)  36.1 us
    all_to_all x1, starting transfers between devices, summed_on_arrival(): blocks = lax.all_to_all(split_up(array, dim, peers), axis, 0, 0, tiled=True)  5.05 us
    unnamed x14, local copies, waits for them, and re-layouts  4.92 us
    dot_general x1, matrix products, on_device(): jnp.dot(flattened, value_weight, preferred_element_type=jnp.float32)  4.87 us
    dot_general x1, matrix products, on_device(): jnp.dot(flattened, key_weight, preferred_element_type=jnp.float32)  4.61 us
  transfers between devices with their start and end apart: 2, of which 2 were waited for; matrix products, arithmetic and copies ran while one was open for 4% of the time, Pallas kernels for 0%

commit v1 on v0

v1 whole, which is shorter than its diff:
```python
import functools

import jax
import jax.numpy as jnp
import numpy as np
from jax import lax
from jax.experimental import pallas as pl
from jax.experimental.pallas import tpu as pltpu
from jax.sharding import PartitionSpec as P

MESH = pl.DeviceIdType.MESH
HEAD_DIM = 64
SUB = 48
NX = 4
VMEM = pl.BlockSpec(memory_space=pltpu.VMEM)
ANY = pl.BlockSpec(memory_space=pl.ANY)


def angle_tables(sp_count):
    lanes = np.arange(128)
    freqs = 10000.0 ** (-2.0 * (lanes % 32) / HEAD_DIM)
    sign = np.where(lanes % HEAD_DIM < HEAD_DIM // 2, -1.0, 1.0)

    def table(positions):
        angles = positions[:, None].astype(np.float64) * freqs[None, :]
        return [np.cos(angles).astype(np.float32), (sign * np.sin(angles)).astype(np.float32)]

    blocks = table(np.arange(sp_count) * (32 * SUB))
    subs = table(np.arange(32) * SUB)
    rows = table(np.arange(SUB))
    return blocks + subs + rows


def kernel(
    x_hbm, wk_hbm, wv_hbm, q_ref, bc, bs, sc, ss, rc, rs,
    k_hbm, v_hbm, part_ref,
    xbuf, wbuf, kst, vst,
    local_sem, lsend, lrecv, dsend, drecv, osem,
):
    sp = lax.axis_index("sp")
    tp = lax.axis_index("tp")
    x, c = tp // 2, lax.rem(tp, 2)
    right = lax.rem(x + 1, NX) * 2 + c
    left = lax.rem(x + NX - 1, NX) * 2 + c
    partner = x * 2 + (1 - c)

    barrier = pltpu.get_barrier_semaphore()
    for peer in (right, left, partner):
        pl.semaphore_signal(barrier, inc=1, device_id={"tp": peer}, device_id_type=MESH)

    mine = [
        pltpu.make_async_copy(x_hbm.at[pl.ds(96 * u, 96)], xbuf.at[u], local_sem.at[u])
        for u in range(2)
    ]
    weights = [
        pltpu.make_async_copy(w, wbuf.at[:, pl.ds(256 * n, 256)], local_sem.at[2 + n])
        for n, w in enumerate((wk_hbm, wv_hbm))
    ]
    for copy in mine + weights:
        copy.start()

    def remote(src, dst, send, recv, peer):
        return pltpu.make_async_remote_copy(
            src_ref=src, dst_ref=dst, send_sem=send, recv_sem=recv,
            device_id={"tp": peer}, device_id_type=MESH,
        )

    def link_copy(src_unit, src_half, q, way):
        return remote(
            xbuf.at[src_unit, pl.ds(SUB * src_half, SUB)],
            xbuf.at[4 + 2 * q, pl.ds(SUB * way, SUB)],
            lsend.at[q, way], lrecv.at[q, way], (right, left)[way],
        )

    def core_copy(unit, to_unit, n):
        return remote(xbuf.at[unit], xbuf.at[to_unit], dsend.at[n], drecv.at[n], partner)

    pl.semaphore_wait(barrier, 3)
    for copy in mine:
        copy.wait()
    for q in range(4):
        for way in range(2):
            s = (q + 2 * way) % 4
            link_copy(s // 2, s % 2, q, way).start()
    for n in range(2):
        core_copy(n, 2 + n, n).start()
    for copy in weights:
        copy.wait()

    lane = lax.broadcasted_iota(jnp.int32, (8, 256), 1)
    row = lax.broadcasted_iota(jnp.int32, (8, 256), 0)
    q_all = jnp.broadcast_to(q_ref[...].astype(jnp.float32), (8, 256))
    q8 = jnp.where(lane // HEAD_DIM == lax.rem(row, 4), q_all, 0.0).astype(jnp.bfloat16)
    base_c, base_s = bc[pl.ds(sp, 1), :], bs[pl.ds(sp, 1), :]
    low_half = lax.rem(lax.broadcasted_iota(jnp.int32, (96, 128), 1), HEAD_DIM) < HEAD_DIM // 2
    upper = lax.broadcasted_iota(jnp.int32, (8, 96), 0) < 4

    def out_copies(unit, places):
        return [
            pltpu.make_async_copy(
                st.at[unit, pl.ds(SUB * j, SUB)],
                hbm.at[pl.ds(places[j] * SUB, SUB)],
                osem.at[unit, 2 * j + n],
            )
            for j in range(2)
            for n, (st, hbm) in enumerate(((kst, k_hbm), (vst, v_hbm)))
        ]

    def compute(unit, places, carry):
        m, l, acc = carry
        raw = jnp.dot(xbuf[unit], wbuf[...], preferred_element_type=jnp.float32)
        cos, sin = [], []
        for place in places:
            c2, s2 = sc[pl.ds(place, 1), :], ss[pl.ds(place, 1), :]
            c12 = base_c * c2 - base_s * s2
            s12 = base_s * c2 + base_c * s2
            cos.append(c12 * rc[...] - s12 * rs[...])
            sin.append(s12 * rc[...] + c12 * rs[...])
        cos, sin = jnp.concatenate(cos, axis=0), jnp.concatenate(sin, axis=0)
        turned = []
        for h in range(2):
            k = raw[:, 128 * h : 128 * h + 128]
            other = jnp.where(low_half, pltpu.roll(k, 96, 1), pltpu.roll(k, 32, 1))
            turned.append((k * cos + other * sin).astype(jnp.bfloat16))
        keys = jnp.concatenate(turned, axis=1)
        values = raw[:, 256:].astype(jnp.bfloat16)
        kst[unit] = keys
        vst[unit] = values
        scores = lax.dot_general(
            q8, keys, (((1,), (1,)), ((), ())), preferred_element_type=jnp.float32
        ) * HEAD_DIM ** (-0.5)
        m_new = jnp.maximum(m, jnp.max(scores, axis=1, keepdims=True))
        p = jnp.exp(scores - m_new)
        alpha = jnp.exp(m - m_new)
        l = l * alpha + jnp.sum(p, axis=1, keepdims=True)
        p_high = p.astype(jnp.bfloat16).astype(jnp.float32)
        p8 = jnp.where(upper, p_high, p - p_high).astype(jnp.bfloat16)
        acc = acc * alpha + jnp.dot(p8, values, preferred_element_type=jnp.float32)
        return m_new, l, acc

    def places_near(u):
        core = lax.rem(c + u // 2, 2)
        first = (2 * x + core) * 4 + 2 * lax.rem(u, 2)
        return first, first + 1

    def places_far(q, core):
        chip_a = lax.rem(x + NX - 1 - q // 4, NX)
        chip_b = lax.rem(x + 1 + q // 4, NX)
        return (2 * chip_a + core) * 4 + lax.rem(q, 4), (2 * chip_b + core) * 4 + lax.rem(q + 2, 4)

    carry = (
        jnp.full((8, 1), -1e30, jnp.float32),
        jnp.zeros((8, 1), jnp.float32),
        jnp.zeros((8, 256), jnp.float32),
    )

    def near(u, carry):
        @pl.when(u >= 2)
        def _():
            core_copy(u - 2, u, u - 2).wait_recv()

        return compute(u, places_near(u), carry)

    carry = lax.fori_loop(0, 4, near, carry)

    def far(q, carry):
        for way in range(2):
            link_copy(0, 0, q, way).wait_recv()

        @pl.when(q < 2)
        def _():
            for way in range(2):
                link_copy(4 + 2 * q, way, q + 4, way).start()

        core_copy(4 + 2 * q, 5 + 2 * q, q + 2).start()

        def one(h, carry):
            @pl.when(h == 1)
            def _():
                core_copy(4 + 2 * q, 5 + 2 * q, q + 2).wait_recv()

            unit = 4 + 2 * q + h
            return compute(unit, places_far(q, lax.rem(c + h, 2)), carry)

        carry = lax.fori_loop(0, 2, one, carry)
        for u in (2 * q, 2 * q + 1):
            @pl.when(u < 4)
            def _(u=u):
                for copy in out_copies(u, places_near(u)):
                    copy.start()

        @pl.when(q >= 2)
        def _():
            for h in range(2):
                for copy in out_copies(2 * q + h, places_far(q - 2, lax.rem(c + h, 2))):
                    copy.start()

        return carry

    m, l, acc = lax.fori_loop(0, 6, far, carry)

    tot = acc[:4] + acc[4:]
    row4 = lax.broadcasted_iota(jnp.int32, (4, 128), 0)
    lane4 = lax.broadcasted_iota(jnp.int32, (4, 128), 1)
    part_ref[0:4] = jnp.where(row4 < 2, tot[:, :128], tot[:, 128:])
    part_ref[4:8] = jnp.where(lane4 < 64, m[:4], l[:4])

    def last_out(n, _):
        q, h = 4 + n // 2, lax.rem(n, 2)
        for copy in out_copies(4 + 2 * q + h, places_far(q, lax.rem(c + h, 2))):
            copy.start()
        return 0

    lax.fori_loop(0, 4, last_out, 0)

    def drain_links(q, _):
        for way in range(2):
            link_copy(0, 0, q, way).wait_send()
        return 0

    lax.fori_loop(0, 6, drain_links, 0)

    def drain_cores(n, _):
        core_copy(0, 0, n).wait_send()
        return 0

    lax.fori_loop(0, 8, drain_cores, 0)

    def drain_out(u, _):
        for copy in out_copies(u, (0, 0)):
            copy.wait()
        return 0

    lax.fori_loop(0, 16, drain_out, 0)


def gathered_read(rows, key_weight, value_weight, queries, tables):
    tables = [jnp.asarray(t) for t in tables]
    count = rows.shape[0] * 8
    return pl.pallas_call(
        kernel,
        out_shape=(
            jax.ShapeDtypeStruct((count, 256), jnp.bfloat16),
            jax.ShapeDtypeStruct((count, 256), jnp.bfloat16),
            jax.ShapeDtypeStruct((8, 128), jnp.float32),
        ),
        in_specs=[ANY, ANY, ANY, VMEM] + [VMEM] * 6,
        out_specs=(ANY, ANY, VMEM),
        scratch_shapes=[
            pltpu.VMEM((16, 96, rows.shape[1]), jnp.bfloat16),
            pltpu.VMEM((rows.shape[1], 512), jnp.bfloat16),
            pltpu.VMEM((16, 96, 256), jnp.bfloat16),
            pltpu.VMEM((16, 96, 256), jnp.bfloat16),
            pltpu.SemaphoreType.DMA((4,)),
            pltpu.SemaphoreType.DMA((6, 2)),
            pltpu.SemaphoreType.DMA((6, 2)),
            pltpu.SemaphoreType.DMA((8,)),
            pltpu.SemaphoreType.DMA((8,)),
            pltpu.SemaphoreType.DMA((16, 4)),
        ],
        compiler_params=pltpu.CompilerParams(collective_id=0, has_side_effects=True),
    )(rows, key_weight, value_weight, queries, *tables)


def copy_for_each(array, axis):
    copies = jnp.broadcast_to(array, (lax.axis_size(axis), *array.shape))
    return lax.all_to_all(copies, axis, split_axis=0, concat_axis=0, tiled=True)


def on_device(layer_input, key_weight, value_weight, new_queries, lambdas, head_gain, out_weight):
    tables = angle_tables(lax.axis_size("sp"))
    keys, values, part = gathered_read(
        layer_input[0], key_weight, value_weight, new_queries, tables
    )
    parts = copy_for_each(part, "sp")
    weighted, highest, totals = parts[:, :4], parts[:, 4:, :1], parts[:, 4:, 64:65]
    factor = jnp.exp(highest - jnp.max(highest, axis=0, keepdims=True))
    reads = jnp.sum(weighted * factor, axis=0) / jnp.sum(totals * factor, axis=0)
    reads = reads.reshape(2, 2, 128)
    diff = reads[:, 0] - lambdas[:, None] * reads[:, 1]
    normed = diff * lax.rsqrt(jnp.mean(diff * diff, axis=-1, keepdims=True) + 1e-06) * head_gain
    headed = normed.reshape(1, -1).astype(jnp.bfloat16)
    partials = jnp.dot(headed, out_weight, preferred_element_type=jnp.float32)
    partials = partials.astype(jnp.bfloat16)
    peers = lax.axis_size("tp")
    blocks = lax.all_to_all(partials.reshape(peers, 1, -1), "tp", 0, 0, tiled=True)
    mixed = jnp.sum(blocks.astype(jnp.float32), axis=0).astype(jnp.bfloat16)
    return keys[None], values[None], mixed


def solution(mesh):
    in_specs = (
        P("gr", ("sp", "tp"), None),
        P(None, "tp"),
        P(None, "tp"),
        P("gr", "tp"),
        P("tp"),
        P(),
        P("tp", None),
    )
    out_specs = (P("gr", "sp", "tp"), P("gr", "sp", "tp"), P("gr", "tp"))
    return jax.shard_map(
        on_device, mesh=mesh, in_specs=in_specs, out_specs=out_specs, check_vma=False
    )
```

time: 144 us -> 96.7 us (0.67)
  waiting for transfers between devices: 62.9 us -> 4.55 us
  Pallas kernels: 0 us -> 42.1 us
  between operations: 14.3 us -> 0.7 us
  matrix products: 10.3 us -> 0.25 us
  local copies, waits for them, and re-layouts: 9.7 us -> 5.12 us
  other arithmetic: 5.04 us -> 1.62 us
  blocking collectives: 36.1 us -> 37.6 us
    all_gather x1 -> x0, waiting for transfers between devices: 61 us -> none  [on_device(): piece = lax.all_gather(layer_input, 'tp', axis=1, tiled=True)]
    pallas_call x0 -> x1, Pallas kernels: none -> 42.1 us  [gathered_read(): pl.pallas_call(kernel, out_shape=(jax.ShapeDtypeStruct((count, 256), jnp....]
    dot_general x4 -> x0, matrix products: 10 us -> none  [the longest x1 4.87 us: on_device(): jnp.dot(flattened, value_weight, preferred_element_type=jnp.float32)]
    all_to_all x1, waiting for transfers between devices: 1.18 us -> 4.55 us  [on_device(): lax.all_to_all(partials.reshape(peers, 1, -1), 'tp', 0, 0, tiled=True)]
    slice x25 -> x1, local copies, waits for them, and re-layouts: 2.3 us -> 0.01 us  [on_device(): diff = reads[:, 0] - lambdas[:, None] * reads[:, 1]]
    unnamed x14 -> x16, local copies, waits for them, and re-layouts: 4.92 us -> 3.14 us
    all_to_all x1, blocking collectives: 36.1 us -> 37.6 us  [copy_for_each(): return lax.all_to_all(copies, axis, split_axis=0, concat_axis=0, tiled=True)]
  transfers between devices with their start and end apart: 2 -> 1, of which waited for: 2 -> 1; matrix products, arithmetic and copies ran while one was open for 4% -> 0% of each run, Pallas kernels for 0% -> 0%
where the time goes in v1:
time: 96.7 us; the launch traced here: 96.3 us
  Pallas kernels  42.1 us (44%)
  blocking collectives  37.6 us (39%)
  local copies, waits for them, and re-layouts  5.12 us (5%)
  waiting for transfers between devices  4.55 us (5%)
  starting transfers between devices  4.41 us (5%)
  other arithmetic  1.62 us (2%)
    pallas_call x1, Pallas kernels, gathered_read(): pl.pallas_call(kernel, out_shape=(jax.ShapeDtypeStruct((count, 256), jnp....  42.1 us
    all_to_all x1, blocking collectives, copy_for_each(): return lax.all_to_all(copies, axis, split_axis=0, concat_axis=0, tiled=True)  37.6 us
    all_to_all x1, waiting for transfers between devices, on_device(): lax.all_to_all(partials.reshape(peers, 1, -1), 'tp', 0, 0, tiled=True)  4.55 us
    all_to_all x1, starting transfers between devices, on_device(): lax.all_to_all(partials.reshape(peers, 1, -1), 'tp', 0, 0, tiled=True)  4.41 us
    unnamed x16, local copies, waits for them, and re-layouts  3.14 us
  transfers between devices with their start and end apart: 1, of which 1 were waited for; matrix products, arithmetic and copies ran while one was open for 0% of the time, Pallas kernels for 0%

profile of v1, /device:TPU:1, one launch (start us, length us, event | category | flops | bytes accessed | tf_op | source)
XLA Modules:
  0.0 96.3 jit_solution(16506971185358646957)
XLA Ops:
  0.6 0.0 copy-start
  0.6 42.1 %shard_map.148 = (bf16[1536,256]{1,0:T(8,128)(2,1)}, bf16[1536,256]{1,0:T(8,128)(2,1)}, f32[8,128]{1,0:T(8,128)}) custom-call(bf16[192,2048]{1,0:T(8,128)(2,1)} %bitcast.29, bf16[2048,256]{1,0:T(8,128)(2,1)} %wk_hbm.1, bf16[2048,256]{1,0:T(8,128)(2,1)} %wv_hbm.1, bf16[1,256]{1,0:T(2,128)(2,1)} %q_ref.1, f32[64,128]{1,0:T(8,128)} %constant.23.clone.bc, ...), custom_call_target="tpu_custom_call" | custom-call | tf_op jit(solution)/shard_map/pallas_call | solution.py:240
  42.7 0.7 broadcast_in_dim.15
  43.4 37.6 %all_to_all.10 = f32[64,8,128]{2,1,0:T(8,128)S(1)} all-to-all(f32[64,8,128]{2,1,0:T(8,128)S(1)} %broadcast_in_dim.15), channel_id=1, replica_groups=mesh['gr'=2,'sp'=64,'tp'=8] {'sp'}, dimensions={0} | all-to-all | bytes 524288 | tf_op jit(solution)/shard_map/all_to_all | solution.py:267
  81.0 0.2 fusion.4
  81.2 0.0 copy-start.3
  81.3 0.0 copy-start.4
  81.3 0.1 copy.36
  81.4 0.0 copy-start.2
  81.4 0.1 copy.37
  81.5 0.2 multiply_reduce_fusion
  81.7 0.1 copy.30
  81.8 0.1 div.14
  81.9 0.1 fusion
  82.0 0.1 broadcast_divide_fusion
  82.1 0.0 copy-done.3
  82.1 0.2 multiply_reduce_fusion.1
  82.3 0.0 copy-done.4
  82.3 0.1 fusion.2
  82.4 0.0 copy-done
  82.4 0.2 fusion.6
  82.7 0.5 broadcast.30
  83.2 0.7 reduce.4
  83.9 0.6 reshape.60
  84.5 4.4 %all-to-all-start.1 = ((bf16[8,2,128]{2,1,0:T(2,128)(2,1)}), bf16[8,2,128]{2,1,0:T(2,128)(2,1)S(1)}, u32[]{:S(2)}, u32[]{:S(2)}) async-start(bf16[8,2,128]{2,1,0:T(2,128)(2,1)} %reshape.60), calls=%async_computation.1 | async-start | bytes 8192 | tf_op jit(solution)/shard_map/all_to_all | solution.py:286
  88.9 4.5 %all-to-all-done.1 = bf16[8,2,128]{2,1,0:T(2,128)(2,1)S(1)} async-done(((bf16[8,2,128]{2,1,0:T(2,128)(2,1)}), bf16[8,2,128]{2,1,0:T(2,128)(2,1)S(1)}, u32[]{:S(2)}, u32[]{:S(2)}) %all-to-all-start.1) | async-done | bytes 4128 | tf_op jit(solution)/shard_map/all_to_all | solution.py:286
  93.5 0.6 reduce_sum.48
  94.0 0.0 copy-done.2
  94.0 0.0 copy-start.1
  94.0 0.9 copy.41
  94.9 0.5 copy-done.1
  95.5 0.9 copy.42
  (7 shorter events, 0.1 us)
Async XLA Ops:
  0.6 81.8 %copy-start = (bf16[256,2048]{1,0:T(8,128)(2,1)S(1)}, bf16[256,2048]{1,0:T(8,128)(2,1)}, u32[]{:S(2)}) copy-start(bf16[256,2048]{1,0:T(8,128)(2,1)} %param.19) | copy-start | bytes 3145732
  81.2 0.8 copy-start.3
  81.3 1.0 %copy-start.4 = (f32[128]{0:T(128)S(1)}, f32[128]{0:T(128)}, u32[]{:S(2)}) copy-start(f32[128]{0:T(128)} %param.18) | copy-start | bytes 1540
  81.4 12.7 %copy-start.2 = (bf16[1536,256]{1,0:T(8,128)(2,1)S(1)}, bf16[1536,256]{1,0:T(8,128)(2,1)}, u32[]{:S(2)}) copy-start(bf16[1536,256]{1,0:T(8,128)(2,1)} %get-tuple-element.6) | copy-start | bytes 2359300
  84.5 9.0 %all-to-all-start.1 = ((bf16[8,2,128]{2,1,0:T(2,128)(2,1)}), bf16[8,2,128]{2,1,0:T(2,128)(2,1)S(1)}, u32[]{:S(2)}, u32[]{:S(2)}) async-start(bf16[8,2,128]{2,1,0:T(2,128)(2,1)} %reshape.60), calls=%async_computation.1 | async-start | bytes 8192 | tf_op jit(solution)/shard_map/all_to_all | solution.py:286
  94.0 1.4 %copy-start.1 = (bf16[1536,256]{1,0:T(8,128)(2,1)S(1)}, bf16[1536,256]{1,0:T(8,128)(2,1)}, u32[]{:S(2)}) copy-start(bf16[1536,256]{1,0:T(8,128)(2,1)} %get-tuple-element.7) | copy-start | bytes 2359300

commit v2 on v1

--- a/solution.py
+++ b/solution.py
@@ -12,6 +12,7 @@
 HEAD_DIM = 64
 SUB = 48
 NX = 4
+NY = 8
 VMEM = pl.BlockSpec(memory_space=pltpu.VMEM)
 ANY = pl.BlockSpec(memory_space=pl.ANY)
 
@@ -32,10 +33,11 @@
 
 
 def kernel(
-    x_hbm, wk_hbm, wv_hbm, q_ref, bc, bs, sc, ss, rc, rs,
-    k_hbm, v_hbm, part_ref,
-    xbuf, wbuf, kst, vst,
+    x_hbm, wk_hbm, wv_hbm, q_ref, lam_ref, gain_ref, wo_hbm, bc, bs, sc, ss, rc, rs,
+    k_hbm, v_hbm, mixed_ref,
+    xbuf, wbuf, obuf, kst, vst, ybuf, zbuf, pbuf, sbuf,
     local_sem, lsend, lrecv, dsend, drecv, osem,
+    ysend, yrecv, zsend, zrecv, psend, precv, token,
 ):
     sp = lax.axis_index("sp")
     tp = lax.axis_index("tp")
@@ -43,10 +45,34 @@
     right = lax.rem(x + 1, NX) * 2 + c
     left = lax.rem(x + NX - 1, NX) * 2 + c
     partner = x * 2 + (1 - c)
+    z, y = sp // NY, lax.rem(sp, NY)
+    depth = lax.axis_size("sp") // NY
+
+    def near_y(step):
+        return z * NY + lax.rem(y + step, NY)
+
+    def tell(sem, step, along_y):
+        if along_y:
+            for way in (step, NY - step):
+                pl.semaphore_signal(sem, inc=1, device_id={"sp": near_y(way)}, device_id_type=MESH)
+
+        @pl.when(z >= step)
+        def _():
+            pl.semaphore_signal(sem, inc=1, device_id={"sp": sp - step * NY}, device_id_type=MESH)
+
+        @pl.when(z + step < depth)
+        def _():
+            pl.semaphore_signal(sem, inc=1, device_id={"sp": sp + step * NY}, device_id_type=MESH)
+
+    def told(step, along_y):
+        below = jnp.where(z >= step, 1, 0)
+        above = jnp.where(z + step < depth, 1, 0)
+        return below + above + (2 if along_y else 0)
 
     barrier = pltpu.get_barrier_semaphore()
     for peer in (right, left, partner):
         pl.semaphore_signal(barrier, inc=1, device_id={"tp": peer}, device_id_type=MESH)
+    tell(barrier, 1, True)
 
     mine = [
         pltpu.make_async_copy(x_hbm.at[pl.ds(96 * u, 96)], xbuf.at[u], local_sem.at[u])
@@ -56,7 +82,8 @@
         pltpu.make_async_copy(w, wbuf.at[:, pl.ds(256 * n, 256)], local_sem.at[2 + n])
         for n, w in enumerate((wk_hbm, wv_hbm))
     ]
-    for copy in mine + weights:
+    projection = pltpu.make_async_copy(wo_hbm, obuf, local_sem.at[4])
+    for copy in mine + weights + [projection]:
         copy.start()
 
     def remote(src, dst, send, recv, peer):
@@ -75,7 +102,7 @@
     def core_copy(unit, to_unit, n):
         return remote(xbuf.at[unit], xbuf.at[to_unit], dsend.at[n], drecv.at[n], partner)
 
-    pl.semaphore_wait(barrier, 3)
+    pl.semaphore_wait(barrier, 3 + told(1, True))
     for copy in mine:
         copy.wait()
     for q in range(4):
@@ -84,6 +111,7 @@
             link_copy(s // 2, s % 2, q, way).start()
     for n in range(2):
         core_copy(n, 2 + n, n).start()
+    tell(token.at[0], 1, True)
     for copy in weights:
         copy.wait()
 
@@ -164,6 +192,16 @@
     carry = lax.fori_loop(0, 4, near, carry)
 
     def far(q, carry):
+        @pl.when(q == 1)
+        def _():
+            pl.semaphore_wait(token.at[0], told(1, True))
+            tell(token.at[1], 2, True)
+
+        @pl.when(q == 3)
+        def _():
+            pl.semaphore_wait(token.at[1], told(2, True))
+            tell(token.at[2], 4, False)
+
         for way in range(2):
             link_copy(0, 0, q, way).wait_recv()
 
@@ -202,8 +240,43 @@
     tot = acc[:4] + acc[4:]
     row4 = lax.broadcasted_iota(jnp.int32, (4, 128), 0)
     lane4 = lax.broadcasted_iota(jnp.int32, (4, 128), 1)
-    part_ref[0:4] = jnp.where(row4 < 2, tot[:, :128], tot[:, 128:])
-    part_ref[4:8] = jnp.where(lane4 < 64, m[:4], l[:4])
+    pl.semaphore_wait(token.at[2], told(4, False))
+
+    def exchange(buf, mine_at, peers, send, recv, axis):
+        return [
+            pltpu.make_async_remote_copy(
+                src_ref=buf.at[mine_at], dst_ref=buf.at[mine_at],
+                send_sem=send.at[n], recv_sem=recv.at[mine_at],
+                device_id={axis: peer}, device_id_type=MESH,
+            )
+            for n, peer in enumerate(peers)
+        ]
+
+    def arrived(buf, slots, send, recv, axis, peer):
+        for slot in slots:
+            pltpu.make_async_remote_copy(
+                src_ref=buf.at[slot], dst_ref=buf.at[slot],
+                send_sem=send.at[0], recv_sem=recv.at[slot],
+                device_id={axis: peer}, device_id_type=MESH,
+            ).wait_recv()
+
+    def packed(weighted, highest, totals):
+        ends = jnp.where(lane4 < 64, highest, totals)
+        return jnp.concatenate([weighted, ends], axis=0)
+
+    def combined(buf):
+        parts = buf[...]
+        highest, totals = parts[:, 4:, 0:1], parts[:, 4:, 64:65]
+        top = jnp.max(highest, axis=0)
+        factor = jnp.exp(highest - top[None])
+        return jnp.sum(parts[:, :4] * factor, axis=0), top, jnp.sum(totals * factor, axis=0)
+
+    ybuf[y] = packed(jnp.where(row4 < 2, tot[:, :128], tot[:, 128:]), m[:4], l[:4])
+    y_slots = [lax.rem(y + k, NY) for k in range(1, NY)]
+    y_peers = [near_y(k) for k in range(1, NY)]
+    y_copies = exchange(ybuf, y, y_peers, ysend, yrecv, "sp")
+    for copy in y_copies:
+        copy.start()
 
     def last_out(n, _):
         q, h = 4 + n // 2, lax.rem(n, 2)
@@ -212,6 +285,15 @@
         return 0
 
     lax.fori_loop(0, 4, last_out, 0)
+    projection.wait()
+    arrived(ybuf, y_slots, ysend, yrecv, "sp", y_peers[0])
+
+    zbuf[z] = packed(*combined(ybuf))
+    z_slots = [lax.rem(z + k, depth) for k in range(1, depth)]
+    z_peers = [slot * NY + y for slot in z_slots]
+    z_copies = exchange(zbuf, z, z_peers, zsend, zrecv, "sp")
+    for copy in z_copies:
+        copy.start()
 
     def drain_links(q, _):
         for way in range(2):
@@ -232,59 +314,84 @@
         return 0
 
     lax.fori_loop(0, 16, drain_out, 0)
-
-
-def gathered_read(rows, key_weight, value_weight, queries, tables):
-    tables = [jnp.asarray(t) for t in tables]
-    count = rows.shape[0] * 8
-    return pl.pallas_call(
+    for copy in y_copies:
+        copy.wait_send()
+    arrived(zbuf, z_slots, zsend, zrecv, "sp", z_peers[0])
+
+    weighted, _, totals = combined(zbuf)
+    reads = weighted / totals
+    headed = []
+    for h in range(2):
+        diff = reads[2 * h : 2 * h + 1] - lam_ref[h] * reads[2 * h + 1 : 2 * h + 2]
+        mean = jnp.mean(diff * diff, axis=1, keepdims=True)
+        headed.append(diff * lax.rsqrt(mean + 1e-06) * gain_ref[...])
+    headed = jnp.broadcast_to(jnp.concatenate(headed, axis=1), (8, 256)).astype(jnp.bfloat16)
+    partial = jnp.dot(headed, obuf[...], preferred_element_type=jnp.float32)
+    partial = partial.astype(jnp.bfloat16).astype(jnp.float32)
+    row8 = lax.broadcasted_iota(jnp.int32, (8, 128), 0)
+    for peer in range(2 * NX):
+        first = 256 * peer
+        sbuf[peer] = jnp.where(
+            row8 == 0, partial[:, first : first + 128], partial[:, first + 128 : first + 256]
+        )
+    p_copies, p_slots = [], []
+    for n in range(1, 2 * NX):
+        peer = lax.rem(tp + n, 2 * NX)
+        p_slots.append(peer)
+        p_copies.append(
+            pltpu.make_async_remote_copy(
+                src_ref=sbuf.at[peer], dst_ref=pbuf.at[tp],
+                send_sem=psend.at[n - 1], recv_sem=precv.at[tp],
+                device_id={"tp": peer}, device_id_type=MESH,
+            )
+        )
+    for copy in p_copies:
+        copy.start()
+    pbuf[tp] = sbuf[tp]
+    for copy in z_copies:
+        copy.wait_send()
+    arrived(pbuf, p_slots, psend, precv, "tp", p_slots[0])
+    total = jnp.sum(pbuf[...], axis=0)
+    mixed_ref[...] = jnp.concatenate([total[0:1], total[1:2]], axis=1).astype(jnp.bfloat16)
+    for copy in p_copies:
+        copy.wait_send()
+
+
+def on_device(layer_input, key_weight, value_weight, new_queries, lambdas, head_gain, out_weight):
+    sp_count = lax.axis_size("sp")
+    rows = layer_input[0]
+    tables = [jnp.asarray(t) for t in angle_tables(sp_count)]
+    count = rows.shape[0] * 2 * NX
+    dma = pltpu.SemaphoreType.DMA
+    keys, values, mixed = pl.pallas_call(
         kernel,
         out_shape=(
             jax.ShapeDtypeStruct((count, 256), jnp.bfloat16),
             jax.ShapeDtypeStruct((count, 256), jnp.bfloat16),
-            jax.ShapeDtypeStruct((8, 128), jnp.float32),
+            jax.ShapeDtypeStruct((1, 256), jnp.bfloat16),
         ),
-        in_specs=[ANY, ANY, ANY, VMEM] + [VMEM] * 6,
+        in_specs=[ANY, ANY, ANY, VMEM, pl.BlockSpec(memory_space=pltpu.SMEM), VMEM, ANY] + [VMEM] * 6,
         out_specs=(ANY, ANY, VMEM),
         scratch_shapes=[
             pltpu.VMEM((16, 96, rows.shape[1]), jnp.bfloat16),
             pltpu.VMEM((rows.shape[1], 512), jnp.bfloat16),
+            pltpu.VMEM(out_weight.shape, jnp.bfloat16),
             pltpu.VMEM((16, 96, 256), jnp.bfloat16),
             pltpu.VMEM((16, 96, 256), jnp.bfloat16),
-            pltpu.SemaphoreType.DMA((4,)),
-            pltpu.SemaphoreType.DMA((6, 2)),
-            pltpu.SemaphoreType.DMA((6, 2)),
-            pltpu.SemaphoreType.DMA((8,)),
-            pltpu.SemaphoreType.DMA((8,)),
-            pltpu.SemaphoreType.DMA((16, 4)),
+            pltpu.VMEM((NY, 8, 128), jnp.float32),
+            pltpu.VMEM((sp_count // NY, 8, 128), jnp.float32),
+            pltpu.VMEM((2 * NX, 8, 128), jnp.float32),
+            pltpu.VMEM((2 * NX, 8, 128), jnp.float32),
+            dma((5,)), dma((6, 2)), dma((6, 2)), dma((8,)), dma((8,)), dma((16, 4)),
+            dma((NY,)), dma((NY,)), dma((sp_count // NY,)), dma((sp_count // NY,)),
+            dma((2 * NX,)), dma((2 * NX,)),
+            pltpu.SemaphoreType.REGULAR((3,)),
         ],
         compiler_params=pltpu.CompilerParams(collective_id=0, has_side_effects=True),
-    )(rows, key_weight, value_weight, queries, *tables)
-
-
-def copy_for_each(array, axis):
-    copies = jnp.broadcast_to(array, (lax.axis_size(axis), *array.shape))
-    return lax.all_to_all(copies, axis, split_axis=0, concat_axis=0, tiled=True)
-
-
-def on_device(layer_input, key_weight, value_weight, new_queries, lambdas, head_gain, out_weight):
-    tables = angle_tables(lax.axis_size("sp"))
-    keys, values, part = gathered_read(
-        layer_input[0], key_weight, value_weight, new_queries, tables
+    )(
+        rows, key_weight, value_weight, new_queries, lambdas, head_gain.reshape(1, -1), out_weight,
+        *tables,
     )
-    parts = copy_for_each(part, "sp")
-    weighted, highest, totals = parts[:, :4], parts[:, 4:, :1], parts[:, 4:, 64:65]
-    factor = jnp.exp(highest - jnp.max(highest, axis=0, keepdims=True))
-    reads = jnp.sum(weighted * factor, axis=0) / jnp.sum(totals * factor, axis=0)
-    reads = reads.reshape(2, 2, 128)
-    diff = reads[:, 0] - lambdas[:, None] * reads[:, 1]
-    normed = diff * lax.rsqrt(jnp.mean(diff * diff, axis=-1, keepdims=True) + 1e-06) * head_gain
-    headed = normed.reshape(1, -1).astype(jnp.bfloat16)
-    partials = jnp.dot(headed, out_weight, preferred_element_type=jnp.float32)
-    partials = partials.astype(jnp.bfloat16)
-    peers = lax.axis_size("tp")
-    blocks = lax.all_to_all(partials.reshape(peers, 1, -1), "tp", 0, 0, tiled=True)
-    mixed = jnp.sum(blocks.astype(jnp.float32), axis=0).astype(jnp.bfloat16)
     return keys[None], values[None], mixed
 
 

time: 96.7 us -> 68.9 us (0.71)
  blocking collectives: 37.6 us -> 0 us
  Pallas kernels: 42.1 us -> 64.4 us
  waiting for transfers between devices: 4.55 us -> 0 us
  starting transfers between devices: 4.41 us -> 0 us
  other arithmetic: 1.62 us -> 0 us
  local copies, waits for them, and re-layouts: 5.12 us -> 3.59 us
    all_to_all x1 -> x0, blocking collectives: 37.6 us -> none  [copy_for_each(): return lax.all_to_all(copies, axis, split_axis=0, concat_axis=0, tiled=True)]
    pallas_call x1, Pallas kernels: 42.1 us -> 64.4 us  [on_device(): pl.pallas_call(kernel, out_shape=(jax.ShapeDtypeStruct((count, 256), jnp....]
    all_to_all x1 -> x0, waiting for transfers between devices: 4.55 us -> none  [on_device(): lax.all_to_all(partials.reshape(peers, 1, -1), 'tp', 0, 0, tiled=True)]
    all_to_all x1 -> x0, starting transfers between devices: 4.41 us -> none  [on_device(): lax.all_to_all(partials.reshape(peers, 1, -1), 'tp', 0, 0, tiled=True)]
    unnamed x16 -> x7, local copies, waits for them, and re-layouts: 3.14 us -> 3.59 us
  transfers between devices with their start and end apart: 1 -> 0, of which waited for: 1 -> 0; matrix products, arithmetic and copies ran while one was open for 0% -> 0% of each run, Pallas kernels for 0% -> 0%
where the time goes in v2:
time: 68.9 us; the launch traced here: 68.7 us
  Pallas kernels  64.4 us (93%)
  local copies, waits for them, and re-layouts  3.59 us (5%)
    pallas_call x1, Pallas kernels, on_device(): pl.pallas_call(kernel, out_shape=(jax.ShapeDtypeStruct((count, 256), jnp....  64.4 us
    unnamed x7, local copies, waits for them, and re-layouts  3.59 us

profile of v2, /device:TPU:1, one launch (start us, length us, event | category | flops | bytes accessed | tf_op | source)
XLA Modules:
  0.0 68.7 jit_solution(6049703619274784383)
XLA Ops:
  0.6 64.4 %shard_map.148 = (bf16[1536,256]{1,0:T(8,128)(2,1)}, bf16[1536,256]{1,0:T(8,128)(2,1)}, bf16[1,256]{1,0:T(2,128)(2,1)}) custom-call(bf16[192,2048]{1,0:T(8,128)(2,1)} %bitcast.4, bf16[2048,256]{1,0:T(8,128)(2,1)} %wk_hbm.1, bf16[2048,256]{1,0:T(8,128)(2,1)} %wv_hbm.1, bf16[1,256]{1,0:T(2,128)(2,1)} %q_ref.1, f32[2]{0:T(128)} %lam_ref.1, f32[1,128]{1,0:T(1,128)} %bitcast.7, ...), custom_call_target="tpu_custom_call" | custom-call | tf_op jit(solution)/shard_map/pallas_call | solution.py:366
  65.1 0.0 copy-start
  65.1 2.1 %copy.19 = bf16[1,1536,256]{2,1,0:T(8,128)(2,1)} copy(bf16[1,1536,256]{2,1,0:T(8,128)(2,1)} %bitcast.6) | data formatting | bytes 1572864
  67.2 0.0 copy-done
  67.2 0.0 copy-start.1
  67.2 0.9 %copy.20 = bf16[1,1536,256]{2,1,0:T(8,128)(2,1)} copy(bf16[1,1536,256]{2,1,0:T(8,128)(2,1)S(1)} %bitcast.5) | data formatting | bytes 1572864
  68.1 0.0 copy-done.1
  68.1 0.6 copy.21
Async XLA Ops:
  65.1 2.1 %copy-start = (bf16[1536,256]{1,0:T(8,128)(2,1)S(1)}, bf16[1536,256]{1,0:T(8,128)(2,1)}, u32[]{:S(2)}) copy-start(bf16[1536,256]{1,0:T(8,128)(2,1)} %get-tuple-element.7) | copy-start | bytes 2359300
  67.2 0.9 %copy-start.1 = (bf16[1,256]{1,0:T(2,128)(2,1)S(1)}, bf16[1,256]{1,0:T(2,128)(2,1)}, u32[]{:S(2)}) copy-start(bf16[1,256]{1,0:T(2,128)(2,1)} %get-tuple-element.14) | copy-start | bytes 1540

commit v3 on v2

v3 whole, which is shorter than its diff:
```python
import jax
import jax.numpy as jnp
import numpy as np
from jax import lax
from jax.experimental import pallas as pl
from jax.experimental.pallas import tpu as pltpu
from jax.sharding import PartitionSpec as P

MESH = pl.DeviceIdType.MESH
HEAD_DIM = 64
GRAIN = 16
UNIT = 96
LATE = 2
PIECE = UNIT // LATE
NX = 4
NY = 8
VMEM = pl.BlockSpec(memory_space=pltpu.VMEM)
ANY = pl.BlockSpec(memory_space=pl.ANY)


def angle_table(sp_count):
    lanes = np.arange(128)
    freqs = 10000.0 ** (-2.0 * (lanes % 32) / HEAD_DIM)
    sign = np.where(lanes % HEAD_DIM < HEAD_DIM // 2, -1.0, 1.0)
    positions = np.concatenate(
        [np.arange(sp_count) * 16 * UNIT, np.arange(16 * UNIT // GRAIN) * GRAIN, np.arange(UNIT)]
    )
    angles = positions[:, None].astype(np.float64) * freqs[None, :]
    return np.concatenate([np.cos(angles), sign * np.sin(angles)], axis=1).astype(np.float32)


def kernel(
    x_hbm, wk_hbm, wv_hbm, q_hbm, lam_hbm, gain_hbm, wo_hbm, table_hbm,
    k_ref, v_ref, mixed_ref,
    xbuf, fbuf, wbuf, obuf, qbuf, gbuf, tbuf, ybuf, zbuf, pbuf, sbuf, lam_ref,
    local_sem, lsend, lrecv, fsend, frecv, dsend, drecv,
    ysend, yrecv, zsend, zrecv, psend, precv, token,
):
    sp = lax.axis_index("sp")
    tp = lax.axis_index("tp")
    x, c = tp // 2, lax.rem(tp, 2)
    right = lax.rem(x + 1, NX) * 2 + c
    left = lax.rem(x + NX - 1, NX) * 2 + c
    partner = x * 2 + (1 - c)
    z, y = sp // NY, lax.rem(sp, NY)
    depth = lax.axis_size("sp") // NY

    def near_y(step):
        return z * NY + lax.rem(y + step, NY)

    def tell(sem, step, along_y):
        if along_y:
            for way in (step, NY - step):
                pl.semaphore_signal(sem, inc=1, device_id={"sp": near_y(way)}, device_id_type=MESH)

        @pl.when(z >= step)
        def _():
            pl.semaphore_signal(sem, inc=1, device_id={"sp": sp - step * NY}, device_id_type=MESH)

        @pl.when(z + step < depth)
        def _():
            pl.semaphore_signal(sem, inc=1, device_id={"sp": sp + step * NY}, device_id_type=MESH)

    def told(step, along_y):
        below = jnp.where(z >= step, 1, 0)
        above = jnp.where(z + step < depth, 1, 0)
        return below + above + (2 if along_y else 0)

    barrier = pltpu.get_barrier_semaphore()
    for peer in (right, left, partner):
        pl.semaphore_signal(barrier, inc=1, device_id={"tp": peer}, device_id_type=MESH)
    tell(barrier, 1, True)

    mine = [
        pltpu.make_async_copy(x_hbm.at[pl.ds(UNIT * u, UNIT)], xbuf.at[u], local_sem.at[u])
        for u in range(2)
    ]
    rest = [
        pltpu.make_async_copy(src, dst, local_sem.at[2 + n])
        for n, (src, dst) in enumerate(
            (
                (wk_hbm, wbuf.at[:, pl.ds(0, 256)]),
                (wv_hbm, wbuf.at[:, pl.ds(256, 256)]),
                (q_hbm, qbuf),
                (table_hbm, tbuf),
                (lam_hbm, lam_ref),
                (gain_hbm, gbuf),
                (wo_hbm, obuf),
            )
        )
    ]
    for copy in mine + rest:
        copy.start()

    def remote(src, dst, send, recv, peer):
        return pltpu.make_async_remote_copy(
            src_ref=src, dst_ref=dst, send_sem=send, recv_sem=recv,
            device_id={"tp": peer}, device_id_type=MESH,
        )

    def link_copy(half, turn, way):
        return remote(
            xbuf.at[half], xbuf.at[4 + 4 * turn + 2 * way],
            lsend.at[turn, way], lrecv.at[turn, way], (right, left)[way],
        )

    def forward_copy(k, way):
        return remote(
            xbuf.at[4 + 2 * way, pl.ds(PIECE * k, PIECE)],
            fbuf.at[2 * k, pl.ds(PIECE * way, PIECE)],
            fsend.at[k, way], frecv.at[k, way], (right, left)[way],
        )

    def core_copy(unit, to_unit, n):
        return remote(xbuf.at[unit], xbuf.at[to_unit], dsend.at[n], drecv.at[n], partner)

    def late_core_copy(k):
        return remote(
            fbuf.at[2 * k], fbuf.at[2 * k + 1], dsend.at[6 + k], drecv.at[6 + k], partner
        )

    for copy in mine:
        copy.wait()
    pl.semaphore_wait(barrier, 3 + told(1, True))
    for turn in range(2):
        for way in range(2):
            link_copy((turn + way) % 2, turn, way).start()
    for n in range(2):
        core_copy(n, 2 + n, n).start()
    tell(token.at[0], 1, True)
    for copy in rest:
        copy.wait()

    lane = lax.broadcasted_iota(jnp.int32, (8, 256), 1)
    row = lax.broadcasted_iota(jnp.int32, (8, 256), 0)
    q_all = jnp.broadcast_to(qbuf[...].astype(jnp.float32), (8, 256))
    q8 = jnp.where(lane // HEAD_DIM == lax.rem(row, 4), q_all, 0.0).astype(jnp.bfloat16)
    sp_count = depth * NY
    base = tbuf[pl.ds(sp, 1), :]
    base_c, base_s = base[:, :128], base[:, 128:]
    sub_count = 16 * UNIT // GRAIN
    rows = tbuf[pl.ds(sp_count + sub_count, UNIT), :]

    def compute(unit_ref, places, carry):
        m, l, acc = carry
        size = unit_ref.shape[0]
        each = size // len(places)
        low_half = lax.rem(lax.broadcasted_iota(jnp.int32, (size, 128), 1), HEAD_DIM) < HEAD_DIM // 2
        upper = lax.broadcasted_iota(jnp.int32, (8, size), 0) < 4
        raw = jnp.dot(unit_ref[...], wbuf[...], preferred_element_type=jnp.float32)
        row_c, row_s = rows[:each, :128], rows[:each, 128:]
        cos, sin = [], []
        for place in places:
            sub = tbuf[pl.ds(sp_count + place, 1), :]
            c2, s2 = sub[:, :128], sub[:, 128:]
            c12 = base_c * c2 - base_s * s2
            s12 = base_s * c2 + base_c * s2
            cos.append(c12 * row_c - s12 * row_s)
            sin.append(s12 * row_c + c12 * row_s)
        cos, sin = jnp.concatenate(cos, axis=0), jnp.concatenate(sin, axis=0)
        turned = []
        for h in range(2):
            k = raw[:, 128 * h : 128 * h + 128]
            other = jnp.where(low_half, pltpu.roll(k, 96, 1), pltpu.roll(k, 32, 1))
            turned.append((k * cos + other * sin).astype(jnp.bfloat16))
        keys = jnp.concatenate(turned, axis=1)
        values = raw[:, 256:].astype(jnp.bfloat16)
        for j, place in enumerate(places):
            at = pl.ds(pl.multiple_of(place * GRAIN, GRAIN), each)
            k_ref[at] = keys[each * j : each * j + each]
            v_ref[at] = values[each * j : each * j + each]
        scores = lax.dot_general(
            q8, keys, (((1,), (1,)), ((), ())), preferred_element_type=jnp.float32
        ) * HEAD_DIM ** (-0.5)
        m_new = jnp.maximum(m, jnp.max(scores, axis=1, keepdims=True))
        p = jnp.exp(scores - m_new)
        alpha = jnp.exp(m - m_new)
        l = l * alpha + jnp.sum(p, axis=1, keepdims=True)
        p_high = p.astype(jnp.bfloat16).astype(jnp.float32)
        p8 = jnp.where(upper, p_high, p - p_high).astype(jnp.bfloat16)
        acc = acc * alpha + jnp.dot(p8, values, preferred_element_type=jnp.float32)
        return m_new, l, acc

    per_piece, per_half, per_late = 2 * UNIT // GRAIN, UNIT // GRAIN, PIECE // GRAIN

    def place_of(chip, core, half):
        return (2 * lax.rem(chip, NX) + core) * per_piece + half * per_half

    carry = (
        jnp.full((8, 1), -1e30, jnp.float32),
        jnp.zeros((8, 1), jnp.float32),
        jnp.zeros((8, 256), jnp.float32),
    )

    def near(u, carry):
        @pl.when(u >= 2)
        def _():
            core_copy(u - 2, u, u - 2).wait_recv()

        core = lax.rem(c + u // 2, 2)
        return compute(xbuf.at[u], [place_of(x, core, lax.rem(u, 2))], carry)

    carry = lax.fori_loop(0, 4, near, carry)
    pl.semaphore_wait(token.at[0], told(1, True))
    tell(token.at[1], 2, True)

    def far(turn, carry):
        @pl.when(turn == 1)
        def _():
            pl.semaphore_wait(token.at[1], told(2, True))
            tell(token.at[2], 4, False)

        for way in range(2):
            link_copy(0, turn, way).wait_recv()

            @pl.when(turn == 0)
            def _(way=way):
                for k in range(LATE):
                    forward_copy(k, way).start()

            core_copy(4 + 4 * turn + 2 * way, 5 + 4 * turn + 2 * way, 2 + 2 * turn + way).start()

        def one(n, carry):
            h, way = n // 2, lax.rem(n, 2)
            unit = 4 + 4 * turn + 2 * way + h

            @pl.when(h == 1)
            def _():
                core_copy(unit - 1, unit, 2 + 2 * turn + way).wait_recv()

            chip = jnp.where(way == 0, x + NX - 1, x + 1)
            place = place_of(chip, lax.rem(c + h, 2), lax.rem(turn + way, 2))
            return compute(xbuf.at[unit], [place], carry)

        return lax.fori_loop(0, 4, one, carry)

    carry = lax.fori_loop(0, 2, far, carry)

    def late(k, carry):
        for way in range(2):
            forward_copy(k, way).wait_recv()
        late_core_copy(k).start()

        def one(h, carry):
            @pl.when(h == 1)
            def _():
                late_core_copy(k).wait_recv()

            core = lax.rem(c + h, 2)
            places = [place_of(x + 2, core, way) + k * per_late for way in range(2)]
            return compute(fbuf.at[2 * k + h], places, carry)

        return lax.fori_loop(0, 2, one, carry)

    m, l, acc = lax.fori_loop(0, LATE, late, carry)

    tot = acc[:4] + acc[4:]
    row4 = lax.broadcasted_iota(jnp.int32, (4, 128), 0)
    lane4 = lax.broadcasted_iota(jnp.int32, (4, 128), 1)
    pl.semaphore_wait(token.at[2], told(4, False))

    def exchange(buf, mine_at, peers, send, recv, axis):
        return [
            pltpu.make_async_remote_copy(
                src_ref=buf.at[mine_at], dst_ref=buf.at[mine_at],
                send_sem=send.at[n], recv_sem=recv.at[mine_at],
                device_id={axis: peer}, device_id_type=MESH,
            )
            for n, peer in enumerate(peers)
        ]

    def arrived(buf, slots, send, recv, axis, peer):
        for slot in slots:
            pltpu.make_async_remote_copy(
                src_ref=buf.at[slot], dst_ref=buf.at[slot],
                send_sem=send.at[0], recv_sem=recv.at[slot],
                device_id={axis: peer}, device_id_type=MESH,
            ).wait_recv()

    def packed(weighted, highest, totals):
        ends = jnp.where(lane4 < 64, highest, totals)
        return jnp.concatenate([weighted, ends], axis=0)

    def combined(buf):
        parts = buf[...]
        highest, totals = parts[:, 4:, 0:1], parts[:, 4:, 64:65]
        top = jnp.max(highest, axis=0)
        factor = jnp.exp(highest - top[None])
        return jnp.sum(parts[:, :4] * factor, axis=0), top, jnp.sum(totals * factor, axis=0)

    ybuf[y] = packed(jnp.where(row4 < 2, tot[:, :128], tot[:, 128:]), m[:4], l[:4])
    y_order = sorted(range(1, NY), key=lambda k: -min(k, NY - k))
    y_slots = [lax.rem(y + k, NY) for k in y_order]
    y_peers = [near_y(k) for k in y_order]
    y_copies = exchange(ybuf, y, y_peers, ysend, yrecv, "sp")
    for copy in y_copies:
        copy.start()

    for way in range(2):
        for turn in range(2):
            link_copy(0, turn, way).wait_send()
        for k in range(LATE):
            forward_copy(k, way).wait_send()
    for n in range(6):
        core_copy(0, 0, n).wait_send()
    for k in range(LATE):
        late_core_copy(k).wait_send()
    arrived(ybuf, y_slots, ysend, yrecv, "sp", y_peers[0])

    zbuf[z] = packed(*combined(ybuf))
    above = depth - 1 - z
    z_slots = [jnp.where(n < above, depth - 1 - n, n - above) for n in range(depth - 1)]
    z_peers = [slot * NY + y for slot in z_slots]
    z_copies = exchange(zbuf, z, z_peers, zsend, zrecv, "sp")
    for copy in z_copies:
        copy.start()
    for copy in y_copies:
        copy.wait_send()
    arrived(zbuf, z_slots, zsend, zrecv, "sp", z_peers[0])

    weighted, _, totals = combined(zbuf)
    reads = weighted / totals
    headed = []
    for h in range(2):
        diff = reads[2 * h : 2 * h + 1] - lam_ref[h] * reads[2 * h + 1 : 2 * h + 2]
        mean = jnp.mean(diff * diff, axis=1, keepdims=True)
        headed.append(diff * lax.rsqrt(mean + 1e-06) * gbuf[...])
    headed = jnp.broadcast_to(jnp.concatenate(headed, axis=1), (8, 256)).astype(jnp.bfloat16)
    partial = jnp.dot(headed, obuf[...], preferred_element_type=jnp.float32)
    partial = partial.astype(jnp.bfloat16).astype(jnp.float32)
    row8 = lax.broadcasted_iota(jnp.int32, (8, 128), 0)
    for peer in range(2 * NX):
        first = 256 * peer
        sbuf[peer] = jnp.where(
            row8 == 0, partial[:, first : first + 128], partial[:, first + 128 : first + 256]
        )
    p_copies, p_slots = [], []
    for n, step in enumerate((4, 5, 3, 2, 6, 7, 1)):
        peer = lax.rem(tp + step, 2 * NX)
        p_slots.append(peer)
        p_copies.append(
            pltpu.make_async_remote_copy(
                src_ref=sbuf.at[peer], dst_ref=pbuf.at[tp],
                send_sem=psend.at[n], recv_sem=precv.at[tp],
                device_id={"tp": peer}, device_id_type=MESH,
            )
        )
    for copy in p_copies:
        copy.start()
    pbuf[tp] = sbuf[tp]
    for copy in z_copies + p_copies:
        copy.wait_send()
    arrived(pbuf, p_slots, psend, precv, "tp", p_slots[0])
    total = jnp.sum(pbuf[...], axis=0)
    mixed_ref[...] = jnp.concatenate([total[0:1], total[1:2]], axis=1).astype(jnp.bfloat16)


def write_out(k_ref, v_ref, mixed_ref, k_hbm, v_hbm, mixed_hbm, sem):
    copies = [
        pltpu.make_async_copy(src, dst, sem.at[n])
        for n, (src, dst) in enumerate(((k_ref, k_hbm), (v_ref, v_hbm), (mixed_ref, mixed_hbm)))
    ]
    for copy in copies:
        copy.start()
    for copy in copies:
        copy.wait()


def on_device(layer_input, key_weight, value_weight, new_queries, lambdas, head_gain, out_weight):
    sp_count = lax.axis_size("sp")
    rows = layer_input[0]
    table = jnp.asarray(angle_table(sp_count))
    shapes = [((rows.shape[0] * 2 * NX, 256), jnp.bfloat16)] * 2 + [((1, 256), jnp.bfloat16)]
    dma = pltpu.SemaphoreType.DMA
    in_vmem = pl.pallas_call(
        kernel,
        out_shape=tuple(pltpu.VMEM(*shape) for shape in shapes),
        in_specs=[ANY] * 8,
        out_specs=(VMEM,) * 3,
        scratch_shapes=[
            pltpu.VMEM((12, UNIT, rows.shape[1]), jnp.bfloat16),
            pltpu.VMEM((2 * LATE, 2 * PIECE, rows.shape[1]), jnp.bfloat16),
            pltpu.VMEM((rows.shape[1], 512), jnp.bfloat16),
            pltpu.VMEM(out_weight.shape, jnp.bfloat16),
            pltpu.VMEM((1, 256), jnp.bfloat16),
            pltpu.VMEM((1, 128), jnp.float32),
            pltpu.VMEM(table.shape, jnp.float32),
            pltpu.VMEM((NY, 8, 128), jnp.float32),
            pltpu.VMEM((sp_count // NY, 8, 128), jnp.float32),
            pltpu.VMEM((2 * NX, 8, 128), jnp.float32),
            pltpu.VMEM((2 * NX, 8, 128), jnp.float32),
            pltpu.SMEM((2,), jnp.float32),
            dma((9,)), dma((2, 2)), dma((2, 2)), dma((LATE, 2)), dma((LATE, 2)),
            dma((6 + LATE,)), dma((6 + LATE,)),
            dma((NY,)), dma((NY,)), dma((sp_count // NY,)), dma((sp_count // NY,)),
            dma((2 * NX,)), dma((2 * NX,)),
            pltpu.SemaphoreType.REGULAR((3,)),
        ],
        compiler_params=pltpu.CompilerParams(collective_id=0, has_side_effects=True),
    )(
        rows, key_weight, value_weight, new_queries, lambdas, head_gain.reshape(1, -1), out_weight,
        table,
    )
    keys, values, mixed = pl.pallas_call(
        write_out,
        out_shape=tuple(jax.ShapeDtypeStruct(*shape) for shape in shapes),
        in_specs=[VMEM] * 3,
        out_specs=(ANY,) * 3,
        scratch_shapes=[dma((3,))],
    )(*(pltpu.with_memory_space_constraint(a, pltpu.VMEM) for a in in_vmem))
    return keys[None], values[None], mixed


def solution(mesh):
    in_specs = (
        P("gr", ("sp", "tp"), None),
        P(None, "tp"),
        P(None, "tp"),
        P("gr", "tp"),
        P("tp"),
        P(),
        P("tp", None),
    )
    out_specs = (P("gr", "sp", "tp"), P("gr", "sp", "tp"), P("gr", "tp"))
    return jax.shard_map(
        on_device, mesh=mesh, in_specs=in_specs, out_specs=out_specs, check_vma=False
    )
```

time: 68.9 us -> 63.5 us (0.922)
  local copies, waits for them, and re-layouts: 3.59 us -> 0 us
  Pallas kernels: 64.4 us -> 62.7 us
    unnamed x7 -> x0, local copies, waits for them, and re-layouts: 3.59 us -> none
    pallas_call x1 -> x2, Pallas kernels: 64.4 us -> 62.7 us  [the longest x1 61.5 us: on_device(): pl.pallas_call(kernel, out_shape=tuple((pltpu.VMEM(*shape) for shape in s...]
where the time goes in v3:
time: 63.5 us; the launch traced here: 63.4 us
  Pallas kernels  62.7 us (99%)
  between operations  0.64 us (1%)
    pallas_call x1, Pallas kernels, on_device(): pl.pallas_call(kernel, out_shape=tuple((pltpu.VMEM(*shape) for shape in s...  61.5 us

profile of v3, /device:TPU:1, one launch (start us, length us, event | category | flops | bytes accessed | tf_op | source)
XLA Modules:
  0.0 63.4 jit_solution(11344501252389991857)
XLA Ops:
  0.6 61.5 %shard_map.103 = (bf16[1536,256]{1,0:T(8,128)(2,1)S(1)}, bf16[1536,256]{1,0:T(8,128)(2,1)S(1)}, bf16[1,256]{1,0:T(2,128)(2,1)S(1)}) custom-call(bf16[192,2048]{1,0:T(8,128)(2,1)} %bitcast.4, bf16[2048,256]{1,0:T(8,128)(2,1)} %wk_hbm.1, bf16[2048,256]{1,0:T(8,128)(2,1)} %wv_hbm.1, bf16[1,256]{1,0:T(2,128)(2,1)} %q_hbm.1, f32[2]{0:T(128)} %lam_hbm.1, ...), custom_call_target="tpu_custom_call" | custom-call | tf_op jit(solution)/shard_map/pallas_call | solution.py:375
  62.2 1.2 %shard_map.104 = (bf16[1536,256]{1,0:T(8,128)(2,1)}, bf16[1536,256]{1,0:T(8,128)(2,1)}, bf16[1,256]{1,0:T(2,128)(2,1)}) custom-call(bf16[1536,256]{1,0:T(8,128)(2,1)S(1)} %get-tuple-element.9.k_ref, bf16[1536,256]{1,0:T(8,128)(2,1)S(1)} %get-tuple-element.10.v_ref, bf16[1,256]{1,0:T(2,128)(2,1)S(1)} %get-tuple-element.11.mixed_ref), custom_call_target="tpu_custom_call" | custom-call | tf_op jit(solution)/shard_map/pallas_call | solution.py:404
